TPU v7x, 512 devices: a whole 4x8x8 slice. The times are simulated.
512 devices in a mesh: sp: 64 (over z, y), fs: 4 (over x), tp: 2 (over core).
Axes of the slice: x: 4, y: 8, z: 8, core: 2. Of those that a mesh axis runs over, the one named last changes fastest.
Arguments:
- tokens: bfloat16 [32768, 2048], P(('fs', 'sp'), 'tp'), parts along dimension 0, may hold values from -450 to 450
- documents: int32 [32768], P(('fs', 'sp')), parts along dimension 0, may hold values from 0 to 7, never falling along the last dimension, each value on 1 to 4096 neighbouring positions
- norm_gain: bfloat16 [2048], P('tp'), may hold values from 0.099609375 to 1.8984375
- out_gate_weight: bfloat16 [2048, 1024], P('sp', 'tp'), may hold values from -0.125 to 0.125
- in_gate_weight: bfloat16 [2048, 1024], P('sp', 'tp'), may hold values from -0.125 to 0.125
- value_weight: bfloat16 [2048, 1024], P('sp', 'tp'), may hold values from -0.125 to 0.125
- conv_taps: bfloat16 [3, 1024], P(None, 'tp'), may hold values from -3.5 to 3.5
- state_in_weight: bfloat16 [2048, 1024], P('sp', 'tp'), may hold values from -0.125 to 0.125
- decay_rate: float32 [64, 64], P('tp'), may hold values from 4e-05 to 2.01
- frequency: float32 [64, 64], P('tp'), may hold values from 0 to 32
- step_log: float32 [64], P('tp'), may hold values from -3.9121 to -1.6094
- input_real: float32 [64, 64, 16], P('tp'), may hold values from -1 to 1
- input_imag: float32 [64, 64, 16], P('tp'), may hold values from -1 to 1
- readout_real: float32 [64, 16, 64], P('tp'), may hold values from -0.75 to 0.75
- readout_imag: float32 [64, 16, 64], P('tp'), may hold values from -0.75 to 0.75
- skip_gain: float32 [1024], P('tp'), may hold values from -4 to 4
- conv_out_weight: bfloat16 [1024, 2048], P('tp', 'sp'), may hold values from -0.125 to 0.125
- state_out_weight: bfloat16 [1024, 2048], P('tp', 'sp'), may hold values from -0.125 to 0.125
Outputs:
- mixed: bfloat16 [32768, 2048], P(('fs', 'sp', 'tp')), parts along dimension 0
There are 4 independent parts, one for each index of `fs`. A program takes and returns all parts, laid end to end along the dimension named above; an argument that names none is the same for every part. Nothing has to cross between parts.
All inputs are finite; a program needn't handle non-finite values.
Results may differ from a plain program's by a relative error of at most 0.015.
Values may be sent and summed in bfloat16 or wider, within the bound.
A program may use at most 64 MiB of HBM per device.

v0:
```python
import math
import jax
import jax.numpy as jnp
from jax import lax
from jax.sharding import Mesh
from jax.sharding import PartitionSpec as P

TAPS = 3
SP = ("sp_0", "sp_1")
FS_SP = ("fs", "sp_0", "sp_1")
FS_SP_TP = ("fs", "sp_0", "sp_1", "tp")
EPS = 1e-06


def rows_first(arrays, axis, dims):
    turned = [jnp.moveaxis(a, dim, 0) for a, dim in zip(arrays, dims)]
    widths = [t[0].size for t in turned]
    both = jnp.concatenate([t.reshape(-1, w) for t, w in zip(turned, widths)], axis=1)
    whole = lax.all_gather(both, axis, axis=0, tiled=True)
    parts = jnp.split(whole, [sum(widths[:k]) for k in range(1, len(widths))], axis=1)
    return tuple(
        (
            jnp.moveaxis(b.reshape(-1, *t.shape[1:]), 0, dim)
            for b, t, dim in zip(parts, turned, dims)
        )
    )


def filled_with(array, identity):
    return jax.tree.map(
        lambda part, zero: jnp.zeros_like(part) + jnp.asarray(zero, part.dtype), array, identity
    )


def gathered_once(array, axis):
    leaves = jax.tree.leaves(array)
    sequence = sorted(range(len(leaves)), key=lambda k: -leaves[k].size)
    width = (1, *leaves[sequence[0]].shape)[-1]
    lines = [
        jnp.pad(leaves[k].reshape(-1), (0, -leaves[k].size % width)).reshape(-1, width)
        for k in sequence
    ]
    both, at, found = (lax.all_gather(jnp.concatenate(lines), axis), 0, {})
    for k, line in zip(sequence, lines):
        section = both[:, at : at + len(line)].reshape(len(both), -1)
        found[k] = section[:, : leaves[k].size].reshape(-1, *leaves[k].shape)
        at += len(line)
    numbers = iter(range(len(leaves)))
    return jax.tree.map(lambda _: found[next(numbers)], array)


def entering(array, axes, combine, identity):
    before = start = filled_with(array, identity)
    total = array
    for axis in reversed(axes):
        devices, here = (lax.axis_size(axis), lax.axis_index(axis))
        pieces = gathered_once(total, axis)
        inside, total = (start, start)
        for k in range(devices):
            passed = k < here
            total = combine(total, jax.tree.map(lambda part: part[k], pieces))
            inside = jax.tree.map(lambda new, old: jnp.where(passed, new, old), total, inside)
        before = combine(inside, before)
    return before


def sent_together(arrays, axis, dim, along):
    widths = [a.shape[along] for a in arrays]
    both = jnp.concatenate(arrays, axis=along)
    whole = lax.all_gather(both, axis, axis=dim, tiled=True)
    return tuple(jnp.split(whole, [sum(widths[:k]) for k in range(1, len(widths))], axis=along))


def from_behind(block, axis, distance):
    devices = range(lax.axis_size(axis))
    route = [(i - distance, i) for i in devices if i - distance in devices]
    return lax.ppermute(block, axis, route)


def cut_along(array, dim, devices):
    shape = array.shape
    parts = array.reshape(*shape[:dim], devices, shape[dim] // devices, *shape[dim + 1 :])
    return jnp.moveaxis(parts, dim, 0)


def summed_on_arrival(array, axis, dim):
    devices = lax.axis_size(axis)
    parts = lax.all_to_all(cut_along(array, dim, devices), axis, 0, 0, tiled=True)
    return jnp.sum(parts.astype(jnp.float32), axis=0)


def chain_step(earlier, later):
    dec_real, dec_imag, end_real, end_imag, first_doc, last_doc = earlier
    late_dec_real, late_dec_imag, late_end_real, late_end_imag, late_first, late_last = later
    joined = (late_first == last_doc) | (last_doc < 0.0) | (late_first < 0.0)
    link = joined.astype(jnp.float32)
    carried_real = late_dec_real * end_real - late_dec_imag * end_imag
    carried_imag = late_dec_real * end_imag + late_dec_imag * end_real
    return (
        link * (late_dec_real * dec_real - late_dec_imag * dec_imag),
        link * (late_dec_real * dec_imag + late_dec_imag * dec_real),
        late_end_real + link * carried_real,
        late_end_imag + link * carried_imag,
        jnp.where(first_doc < 0.0, late_first, first_doc),
        jnp.where(late_last < 0.0, last_doc, late_last),
    )


def ssm_constants(decay_rate, frequency, step_log, input_real, input_imag):
    step_size = jnp.exp(step_log)[:, None]
    damping = decay_rate * step_size
    turning = frequency * step_size
    fading = jnp.exp(-damping)
    coef_imag = fading * jnp.sin(turning)
    half_sine = jnp.sin(turning / 2.0)
    less_real = jnp.expm1(-damping) * jnp.cos(turning) - 2.0 * half_sine * half_sine
    denominator = decay_rate * decay_rate + frequency * frequency
    ratio_real = (-less_real * decay_rate + coef_imag * frequency) / denominator
    ratio_imag = (-coef_imag * decay_rate - less_real * frequency) / denominator
    bbar_real = ratio_real[..., None] * input_real - ratio_imag[..., None] * input_imag
    bbar_imag = ratio_real[..., None] * input_imag + ratio_imag[..., None] * input_real
    return (bbar_real, bbar_imag, damping.reshape(-1), turning.reshape(-1))


def block_recurrence(
    damping,
    turning,
    bbar_real,
    bbar_imag,
    driven,
    keep_rows,
    doc_rows,
    carry_real,
    carry_imag,
    readout_real,
    readout_imag,
):
    groups, group_size, state_size = readout_real.shape
    row_count = driven.shape[0]
    block = math.gcd(row_count, 16)
    blocks = row_count // block
    steps = jnp.arange(block, dtype=jnp.float32)
    gap = steps[:, None] - steps[None, :]
    lower = (gap >= 0.0).astype(jnp.float32)
    gap_pos = jnp.maximum(gap, 0.0)[:, :, None]
    pair_fade = jnp.exp(-gap_pos * damping[None, None, :])
    pair_real = pair_fade * jnp.cos(gap_pos * turning[None, None, :])
    pair_imag = pair_fade * jnp.sin(gap_pos * turning[None, None, :])
    lead = (steps + 1.0)[:, None]
    lead_fade = jnp.exp(-lead * damping[None, :])
    lead_real = lead_fade * jnp.cos(lead * turning[None, :])
    lead_imag = lead_fade * jnp.sin(lead * turning[None, :])

    def one_block(carry, pieces):
        start_real, start_imag = carry
        inputs, keeps, docs = pieces
        split_rows = inputs.reshape(block, groups, group_size)
        push_real = jnp.einsum("tgh,gph->tgp", split_rows, bbar_real).reshape(
            block, groups * state_size
        )
        push_imag = jnp.einsum("tgh,gph->tgp", split_rows, bbar_imag).reshape(
            block, groups * state_size
        )
        same = lower * (docs[:, None] == docs[None, :]).astype(jnp.float32)
        weigh_real = same[:, :, None] * pair_real
        weigh_imag = same[:, :, None] * pair_imag
        alive = (keeps[0] * (docs == docs[0]).astype(jnp.float32))[:, None]
        held_real = jnp.sum(
            weigh_real * push_real[None, :, :] - weigh_imag * push_imag[None, :, :], axis=1
        ) + alive * (lead_real * start_real[None, :] - lead_imag * start_imag[None, :])
        held_imag = jnp.sum(
            weigh_real * push_imag[None, :, :] + weigh_imag * push_real[None, :, :], axis=1
        ) + alive * (lead_real * start_imag[None, :] + lead_imag * start_real[None, :])
        result = jnp.einsum(
            "tgp,ghp->tgh", held_real.reshape(block, groups, state_size), readout_real
        )
        result = result - jnp.einsum(
            "tgp,ghp->tgh", held_imag.reshape(block, groups, state_size), readout_imag
        )
        return ((held_real[-1], held_imag[-1]), result.reshape(block, groups * group_size))

    _, outputs = lax.scan(
        one_block,
        (carry_real, carry_imag),
        (
            driven.reshape(blocks, block, -1),
            keep_rows.reshape(blocks, block),
            doc_rows.reshape(blocks, block),
        ),
    )
    return outputs.reshape(row_count, groups * group_size)


def shards(
    tokens,
    documents,
    norm_gain,
    out_gate_weight,
    in_gate_weight,
    value_weight,
    conv_taps,
    state_in_weight,
    decay_rate,
    frequency,
    step_log,
    input_real,
    input_imag,
    readout_real,
    readout_imag,
    skip_gain,
    conv_out_weight,
    state_out_weight,
):
    row_count = tokens.shape[0]
    groups, state_size = decay_rate.shape
    group_size = input_real.shape[2]
    whole, gains = rows_first((tokens, norm_gain), "tp", (1, 0))
    values = whole.astype(jnp.float32)
    scale = lax.rsqrt(jnp.mean(values * values, axis=1, keepdims=True) + EPS)
    normed = (values * scale * gains.astype(jnp.float32)[None, :]).astype(jnp.bfloat16)

    def add_rows(pieces):
        return tuple(
            (jnp.dot(normed, piece, preferred_element_type=jnp.float32) for piece in pieces)
        )

    bbar_real, bbar_imag, damping, turning = ssm_constants(
        decay_rate, frequency, step_log, input_real, input_imag
    )
    doc_float = documents.astype(jnp.float32)
    (driven_sum,) = add_rows((lax.all_gather(state_in_weight, SP, axis=0, tiled=True),))
    driven_wide = driven_sum.astype(jnp.bfloat16).astype(jnp.float32)
    split_rows = driven_wide.reshape(row_count, groups, group_size)
    backward = (row_count - 1 - jnp.arange(row_count)).astype(jnp.float32)[:, None]
    alive = (documents == documents[-1]).astype(jnp.float32)[:, None]
    fading = jnp.exp(-backward * damping[None, :]) * alive
    weigh_real = (fading * jnp.cos(backward * turning[None, :])).reshape(
        row_count, groups, state_size
    )
    weigh_imag = (fading * jnp.sin(backward * turning[None, :])).reshape(
        row_count, groups, state_size
    )
    moment_real = jnp.einsum("tgp,tgh->gph", weigh_real, split_rows)
    moment_imag = jnp.einsum("tgp,tgh->gph", weigh_imag, split_rows)
    end_real = jnp.sum(bbar_real * moment_real - bbar_imag * moment_imag, axis=2).reshape(-1)
    end_imag = jnp.sum(bbar_real * moment_imag + bbar_imag * moment_real, axis=2).reshape(-1)
    whole_doc = (documents[0] == documents[-1]).astype(jnp.float32)
    total_fade = jnp.exp(-row_count * damping) * whole_doc
    element = (
        total_fade * jnp.cos(row_count * turning),
        total_fade * jnp.sin(row_count * turning),
        end_real,
        end_imag,
        doc_float[:1],
        doc_float[-1:],
    )
    identity = (
        jnp.ones_like(end_real),
        jnp.zeros_like(end_real),
        jnp.zeros_like(end_real),
        jnp.zeros_like(end_real),
        jnp.full((1,), -1.0, jnp.float32),
        jnp.full((1,), -1.0, jnp.float32),
    )
    incoming = entering(element, SP, chain_step, identity)
    driven_wide, incoming = (driven_wide, incoming)
    gate_sum, inner_sum, value_sum = add_rows(
        sent_together((out_gate_weight, in_gate_weight, value_weight), SP, 0, 1)
    )
    out_gate = gate_sum.astype(jnp.bfloat16).astype(jnp.float32)
    in_gate = inner_sum.astype(jnp.bfloat16).astype(jnp.float32)
    value = value_sum.astype(jnp.bfloat16).astype(jnp.float32)
    product = (in_gate * value).astype(jnp.bfloat16)
    margin = TAPS - 1
    tail_same = documents[row_count - margin :] == documents[-1]
    tail_rows = jnp.where(
        tail_same[:, None], product[row_count - margin :], jnp.zeros_like(product[:margin])
    )
    rim_rows = from_behind(tail_rows, SP, 1)
    in_dec_real, in_dec_imag, in_real, in_imag, in_first, in_last = incoming
    padded = jnp.concatenate([rim_rows, product], axis=0)
    padded_docs = jnp.concatenate([jnp.broadcast_to(in_last, (margin,)), doc_float], axis=0)
    total = jnp.zeros(product.shape, jnp.float32)
    for index in range(TAPS):
        same_doc = (padded_docs[index : index + row_count] == doc_float).astype(jnp.float32)
        total = (
            total
            + conv_taps[index].astype(jnp.float32)[None, :]
            * padded[index : index + row_count].astype(jnp.float32)
            * same_doc[:, None]
        )
    conv_out = (out_gate * total).astype(jnp.bfloat16)
    link_first = (in_last == doc_float[:1]).astype(jnp.float32)
    keep_rows = jnp.concatenate(
        [link_first, (documents[1:] == documents[:-1]).astype(jnp.float32)], axis=0
    )
    readout = block_recurrence(
        damping,
        turning,
        bbar_real,
        bbar_imag,
        driven_wide,
        keep_rows,
        doc_float,
        in_real,
        in_imag,
        readout_real,
        readout_imag,
    )
    ssm_out = jax.nn.gelu(readout + skip_gain[None, :] * driven_wide, approximate=True).astype(
        jnp.bfloat16
    )
    conv_columns, state_columns = rows_first((conv_out_weight, state_out_weight), SP, (1, 1))
    summed = summed_on_arrival(
        (
            jnp.dot(conv_out, conv_columns, preferred_element_type=jnp.float32)
            + jnp.dot(ssm_out, state_columns, preferred_element_type=jnp.float32)
        ).astype(jnp.bfloat16),
        "tp",
        0,
    )
    return summed.astype(jnp.bfloat16)


def solution(mesh):
    torus = Mesh(
        mesh.devices.reshape(8, 8, mesh.shape["fs"], mesh.shape["tp"]), ("sp_0", "sp_1", "fs", "tp")
    )
    in_specs = (
        P(FS_SP, "tp"),
        P(FS_SP),
        P("tp"),
        P(SP, "tp"),
        P(SP, "tp"),
        P(SP, "tp"),
        P(None, "tp"),
        P(SP, "tp"),
        P("tp", None),
        P("tp", None),
        P("tp"),
        P("tp", None, None),
        P("tp", None, None),
        P("tp", None, None),
        P("tp", None, None),
        P("tp"),
        P("tp", SP),
        P("tp", SP),
    )
    out_specs = P(FS_SP_TP, None)
    return jax.shard_map(
        shards, mesh=torus, in_specs=in_specs, out_specs=out_specs, check_vma=False
    )
```

profile of v0, /device:TPU:67, one launch (start us, length us, event | category | flops | bytes accessed | tf_op | source)
XLA Modules:
  0.0 351.8 jit_solution(8348065107115574287)
XLA Ops:
  6.6 0.7 all-gather.10.cloned.1.call-update
  7.4 1.4 pad_maximum_fusion.3
  8.9 1.4 pad_maximum_fusion.4
  10.3 0.7 reshape.1674
  11.0 1.0 pad_maximum_fusion
  12.0 2.5 all_gather.24
  14.7 0.6 fusion.204
  15.4 0.6 fusion.203
  16.1 0.6 compare_convert_fusion.3
  16.7 0.7 slice_compare_fusion.1
  18.7 0.3 fusion.120
  19.1 0.6 pad.14
  19.7 0.5 pad.15
  20.6 72.3 %all-gather.10.cloned.1.call-done = bf16[2048,512]{1,0:T(8,128)(2,1)} async-done(((bf16[32,512]{1,0:T(8,128)(2,1)}), bf16[2048,512]{1,0:T(8,128)(2,1)}) %all-gather.10.cloned.1.call-update) | async-done | bytes 2097168 | tf_op jit(solution)/shard_map/all_gather | solution.py:231
  92.8 2.1 convolution_convert_fusion
  95.0 3.8 %fusion.79 = f32[32,64,16]{1,2,0:T(8,128)S(1)} fusion(bf16[128,32,16]{0,2,1:T(8,128)(2,1)S(1)} %bitcast.596, f32[32,64]{1,0:T(8,128)S(1)} %get-tuple-element.406, f32[128]{0:T(128)S(1)} %subtract_convert_fusion, f32[128]{0:T(128)S(1)} %get-tuple-element.414, f32[32,64]{1,0:T(8,128)S(1)} %get-tuple-element.405, f32[128]{0:T(128)S(1)} %fusion.178), kind=kOutput, calls=%fused_computation.77 | convolution fusion | flops 9437184 | bytes 280064 | tf_op jit(solution)/shard_map/tgp,tgh->gph/dot_general | solution.py:244
  98.8 4.4 %add_reduce_fusion = (f32[32,64]{1,0:T(8,128)S(1)}, f32[32,64]{1,0:T(8,128)S(1)}) fusion(f32[32,64,16]{1,2,0:T(8,128)S(1)} %get-tuple-element.304, f32[32,64,16]{1,2,0:T(8,128)S(1)} %get-tuple-element.253, f32[32,64,16]{1,2,0:T(8,128)S(1)} %fusion.79, bf16[128,32,16]{0,2,1:T(8,128)(2,1)S(1)} %bitcast.597, f32[32,64]{1,0:T(8,128)S(1)} %get-tuple-element.406, ...), kind=kOutput, calls=%fused_computation.109 | convolution fusion | flops 9695232 | bytes 558592 | tf_op jit(solution)/shard_map/tgp,tgh->gph/dot_general | solution.py:243
  103.5 20.1 %all-gather.2 = f32[8,6,2048]{2,1,0:T(8,128)S(1)} all-gather(f32[1,6,2048]{2,1,0:T(8,128)S(1)} %bitcast.593), channel_id=2, replica_groups=mesh['sp_0'=8,'sp_1'=8,'fs'=4,'tp'=2] {'sp_1'}, dimensions={0}, use_global_device_ids=true | all-gather | bytes 442368 | tf_op jit(solution)/shard_map/all_gather | solution.py:43
  123.7 0.6 fusion.201
  124.3 0.6 fusion.202
  150.5 23.6 %all-gather.3 = f32[8,6,2048]{2,1,0:T(8,128)S(1)} all-gather(f32[1,6,2048]{2,1,0:T(8,128)S(1)} %bitcast.594), channel_id=3, replica_groups=mesh['sp_0'=8,'sp_1'=8,'fs'=4,'tp'=2] {'sp_0'}, dimensions={0}, use_global_device_ids=true | all-gather | bytes 442368 | tf_op jit(solution)/shard_map/all_gather | solution.py:43
  174.3 0.6 fusion.200
  180.2 0.6 fusion.199
  197.1 111.0 %while.16 = (s32[]{:T(128)}, f32[2048]{0:T(1024)S(1)}, f32[2048]{0:T(1024)S(1)}, f32[8,16,512]{2,1,0:T(8,128)S(1)}, f32[8,16]{1,0:T(8,128)S(1)}, /*index=5*/bf16...) while((s32[]{:T(128)}, f32[2048]{0:T(1024)S(1)}, ...), condition=%wide.region_6.7_spmd.clone.clone, body=%wide.region_3.6_spmd.clone.clone.sunk | while | flops 12023074 | bytes 4772677 | solution.py:182
  198.2 9.6 %fusion.233 = (f32[16,2048]{1,0:T(8,128)S(1)}, f32[16,2048]{1,0:T(8,128)S(1)}) fusion(f32[2048]{0:T(1024)S(1)} %get-tuple-element.596, f32[16,16]{1,0:T(8,128)S(1)} %get-tuple-element.597, f32[2048]{0:T(1024)S(1)} %get-tuple-element.594, f32[16,16]{1,0:T(8,128)S(1)} %get-tuple-element.595, f32[16,2048]{1,0:T(8,128)S(1)} %mul.4733, ...), kind=kLoop, calls=%fused_computation.19.clone.1 | loop fusion | flops 7274496 | bytes 543744 | tf_op jit(solution)/shard_map/while/body/eval_jaxpr/reduce_sum | solution.py:171
  208.1 0.6 fusion.234
  209.8 0.6 slice.1072
  210.4 0.6 slice_add_fusion.18
  212.1 9.6 %fusion.233 = (f32[16,2048]{1,0:T(8,128)S(1)}, f32[16,2048]{1,0:T(8,128)S(1)}) fusion(f32[2048]{0:T(1024)S(1)} %get-tuple-element.596, f32[16,16]{1,0:T(8,128)S(1)} %get-tuple-element.597, f32[2048]{0:T(1024)S(1)} %get-tuple-element.594, f32[16,16]{1,0:T(8,128)S(1)} %get-tuple-element.595, f32[16,2048]{1,0:T(8,128)S(1)} %mul.4733, ...), kind=kLoop, calls=%fused_computation.19.clone.1 | loop fusion | flops 7274496 | bytes 543744 | tf_op jit(solution)/shard_map/while/body/eval_jaxpr/reduce_sum | solution.py:171
  222.0 0.6 fusion.234
  223.7 0.6 slice.1072
  224.3 0.6 slice_add_fusion.18
  226.0 9.6 %fusion.233 = (f32[16,2048]{1,0:T(8,128)S(1)}, f32[16,2048]{1,0:T(8,128)S(1)}) fusion(f32[2048]{0:T(1024)S(1)} %get-tuple-element.596, f32[16,16]{1,0:T(8,128)S(1)} %get-tuple-element.597, f32[2048]{0:T(1024)S(1)} %get-tuple-element.594, f32[16,16]{1,0:T(8,128)S(1)} %get-tuple-element.595, f32[16,2048]{1,0:T(8,128)S(1)} %mul.4733, ...), kind=kLoop, calls=%fused_computation.19.clone.1 | loop fusion | flops 7274496 | bytes 543744 | tf_op jit(solution)/shard_map/while/body/eval_jaxpr/reduce_sum | solution.py:171
  235.8 0.6 fusion.234
  237.6 0.6 slice.1072
  238.2 0.6 slice_add_fusion.18
  239.9 9.6 %fusion.233 = (f32[16,2048]{1,0:T(8,128)S(1)}, f32[16,2048]{1,0:T(8,128)S(1)}) fusion(f32[2048]{0:T(1024)S(1)} %get-tuple-element.596, f32[16,16]{1,0:T(8,128)S(1)} %get-tuple-element.597, f32[2048]{0:T(1024)S(1)} %get-tuple-element.594, f32[16,16]{1,0:T(8,128)S(1)} %get-tuple-element.595, f32[16,2048]{1,0:T(8,128)S(1)} %mul.4733, ...), kind=kLoop, calls=%fused_computation.19.clone.1 | loop fusion | flops 7274496 | bytes 543744 | tf_op jit(solution)/shard_map/while/body/eval_jaxpr/reduce_sum | solution.py:171
  249.7 0.6 fusion.234
  251.5 0.6 slice.1072
  252.0 0.6 slice_add_fusion.18
  253.8 9.6 %fusion.233 = (f32[16,2048]{1,0:T(8,128)S(1)}, f32[16,2048]{1,0:T(8,128)S(1)}) fusion(f32[2048]{0:T(1024)S(1)} %get-tuple-element.596, f32[16,16]{1,0:T(8,128)S(1)} %get-tuple-element.597, f32[2048]{0:T(1024)S(1)} %get-tuple-element.594, f32[16,16]{1,0:T(8,128)S(1)} %get-tuple-element.595, f32[16,2048]{1,0:T(8,128)S(1)} %mul.4733, ...), kind=kLoop, calls=%fused_computation.19.clone.1 | loop fusion | flops 7274496 | bytes 543744 | tf_op jit(solution)/shard_map/while/body/eval_jaxpr/reduce_sum | solution.py:171
  263.6 0.6 fusion.234
  265.3 0.6 slice.1072
  265.9 0.6 slice_add_fusion.18
  267.6 9.6 %fusion.233 = (f32[16,2048]{1,0:T(8,128)S(1)}, f32[16,2048]{1,0:T(8,128)S(1)}) fusion(f32[2048]{0:T(1024)S(1)} %get-tuple-element.596, f32[16,16]{1,0:T(8,128)S(1)} %get-tuple-element.597, f32[2048]{0:T(1024)S(1)} %get-tuple-element.594, f32[16,16]{1,0:T(8,128)S(1)} %get-tuple-element.595, f32[16,2048]{1,0:T(8,128)S(1)} %mul.4733, ...), kind=kLoop, calls=%fused_computation.19.clone.1 | loop fusion | flops 7274496 | bytes 543744 | tf_op jit(solution)/shard_map/while/body/eval_jaxpr/reduce_sum | solution.py:171
  277.5 0.6 fusion.234
  279.2 0.6 slice.1072
  279.8 0.6 slice_add_fusion.18
  281.5 9.6 %fusion.233 = (f32[16,2048]{1,0:T(8,128)S(1)}, f32[16,2048]{1,0:T(8,128)S(1)}) fusion(f32[2048]{0:T(1024)S(1)} %get-tuple-element.596, f32[16,16]{1,0:T(8,128)S(1)} %get-tuple-element.597, f32[2048]{0:T(1024)S(1)} %get-tuple-element.594, f32[16,16]{1,0:T(8,128)S(1)} %get-tuple-element.595, f32[16,2048]{1,0:T(8,128)S(1)} %mul.4733, ...), kind=kLoop, calls=%fused_computation.19.clone.1 | loop fusion | flops 7274496 | bytes 543744 | tf_op jit(solution)/shard_map/while/body/eval_jaxpr/reduce_sum | solution.py:171
  291.4 0.6 fusion.234
  293.1 0.6 slice.1072
  293.7 0.6 slice_add_fusion.18
  295.4 9.6 %fusion.233 = (f32[16,2048]{1,0:T(8,128)S(1)}, f32[16,2048]{1,0:T(8,128)S(1)}) fusion(f32[2048]{0:T(1024)S(1)} %get-tuple-element.596, f32[16,16]{1,0:T(8,128)S(1)} %get-tuple-element.597, f32[2048]{0:T(1024)S(1)} %get-tuple-element.594, f32[16,16]{1,0:T(8,128)S(1)} %get-tuple-element.595, f32[16,2048]{1,0:T(8,128)S(1)} %mul.4733, ...), kind=kLoop, calls=%fused_computation.19.clone.1 | loop fusion | flops 7274496 | bytes 543744 | tf_op jit(solution)/shard_map/while/body/eval_jaxpr/reduce_sum | solution.py:171
  305.2 0.6 fusion.234
  307.0 0.6 slice.1072
  307.6 0.6 slice_add_fusion.18
  308.3 2.1 fusion.67
  310.4 2.1 fusion.61
  312.6 1.9 collective-permute-start
  314.6 4.4 %collective-permute-done = bf16[2,512]{1,0:T(2,128)(2,1)S(1)} collective-permute-done((bf16[2,512]{1,0:T(2,128)(2,1)S(1)}, bf16[2,512]{1,0:T(2,128)(2,1)S(1)}, u32[]{:S(2)}, u32[]{:S(2)}) %collective-permute-start) | collective-permute-done | bytes 2080 | tf_op jit(solution)/shard_map/ppermute | solution.py:77
  319.0 3.4 fusion.32
  322.5 2.4 fusion.30
  324.9 19.6 %all_to_all.5 = bf16[2,64,2048]{2,1,0:T(8,128)(2,1)S(1)} all-to-all(bf16[2,64,2048]{2,1,0:T(8,128)(2,1)S(1)} %bitcast.586), channel_id=1, replica_groups=mesh['sp_0'=8,'sp_1'=8,'fs'=4,'tp'=2] {'tp'}, dimensions={0} | all-to-all | bytes 1048576 | tf_op jit(solution)/shard_map/all_to_all | solution.py:88
  344.5 0.8 reduce_sum.64
  (284 shorter events, 22.8 us)
Async XLA Ops:
  6.5 8.2 %copy-start.7 = (s32[128]{0:T(128)S(1)}, s32[128]{0:T(128)}, u32[]{:S(2)}) copy-start(s32[128]{0:T(128)} %param.21) | copy-start | bytes 1540
  6.5 12.1 %copy-start.9 = (f32[32]{0:T(128)S(1)}, f32[32]{0:T(128)}, u32[]{:S(2)}) copy-start(f32[32]{0:T(128)} %param.30) | copy-start | bytes 388
  6.5 12.1 %copy-start.5 = (f32[32,64]{1,0:T(8,128)S(1)}, f32[32,64]{1,0:T(8,128)}, u32[]{:S(2)}) copy-start(f32[32,64]{1,0:T(8,128)} %param.28) | copy-start | bytes 24580
  6.5 12.1 %copy-start.4 = (f32[32,64]{1,0:T(8,128)S(1)}, f32[32,64]{1,0:T(8,128)}, u32[]{:S(2)}) copy-start(f32[32,64]{1,0:T(8,128)} %param.29) | copy-start | bytes 24580
  6.5 13.8 %copy-start = (f32[32,16,64]{2,1,0:T(8,128)S(1)}, f32[32,16,64]{2,1,0:T(8,128)}, u32[]{:S(2)}) copy-start(f32[32,16,64]{2,1,0:T(8,128)} %param.33) | copy-start | bytes 393220
  6.5 13.9 %copy-start.1 = (f32[32,16,64]{2,1,0:T(8,128)S(1)}, f32[32,16,64]{2,1,0:T(8,128)}, u32[]{:S(2)}) copy-start(f32[32,16,64]{2,1,0:T(8,128)} %param.34) | copy-start | bytes 393220
  6.6 13.9 %copy-start.6 = (bf16[3,512]{1,0:T(4,128)(2,1)S(1)}, bf16[3,512]{1,0:T(4,128)(2,1)}, u32[]{:S(2)}) copy-start(bf16[3,512]{1,0:T(4,128)(2,1)} %param.26) | copy-start | bytes 9220
  6.6 13.9 %copy-start.3 = (f32[32,64,16]{1,2,0:T(8,128)S(1)}, f32[32,64,16]{1,2,0:T(8,128)}, u32[]{:S(2)}) copy-start(f32[32,64,16]{1,2,0:T(8,128)} %param.31) | copy-start | bytes 393220
  6.6 13.9 %copy-start.2 = (f32[32,64,16]{1,2,0:T(8,128)S(1)}, f32[32,64,16]{1,2,0:T(8,128)}, u32[]{:S(2)}) copy-start(f32[32,64,16]{1,2,0:T(8,128)} %param.32) | copy-start | bytes 393220
  6.6 86.2 %all-gather.10.cloned.1.call-start = ((), (), s32[]{:S(2)}) async-start(), calls=%async_computation.2 | async-start | bytes 2129920 | tf_op jit(solution)/shard_map/all_gather | solution.py:231
  7.3 301.0 %all-gather.8.cloned.1.call-start = ((), (), s32[]{:S(2)}) async-start(), calls=%async_computation.1 | async-start | bytes 6389760 | tf_op jit(solution)/shard_map/all_gather | solution.py:70
  8.8 305.7 %all-gather.12.cloned.1.call-start = ((), (), s32[]{:S(2)}) async-start(), calls=%async_computation.3 | async-start | bytes 4259840 | tf_op jit(solution)/shard_map/all_gather | solution.py:19
  197.1 111.0 %copy-start.8 = (f32[512]{0:T(512)S(1)}, f32[512]{0:T(512)}, u32[]{:S(2)}) copy-start(f32[512]{0:T(512)} %param.35) | copy-start | bytes 6148
  312.6 6.4 %collective-permute-start = (bf16[2,512]{1,0:T(2,128)(2,1)S(1)}, bf16[2,512]{1,0:T(2,128)(2,1)S(1)}, u32[]{:S(2)}, u32[]{:S(2)}) collective-permute-start(bf16[2,512]{1,0:T(2,128)(2,1)S(1)} %broadcast_select_fusion.8), channel_id=1, source_target_pairs={{0,8},{8,16},{16,24},{24,32},{32,40},{40,48},{48,56},{56,64},{64,7... | collective-permute-start | bytes 6152 | tf_op jit(solution)/shard_map/ppermute | solution.py:77
Sparse Core Ops, SparseCore 0:
  10.5 82.3 all-gather.9
  95.8 93.9 all-gather.7
  192.9 81.4 all-gather.11
where the time goes:
time: 353 us; the launch traced here: 352 us
  other arithmetic  96.2 us (27%)
  waiting for transfers between devices  77.4 us (22%)
  blocking collectives  65.8 us (19%)
  between operations  60.3 us (17%)
  matrix products  26.4 us (7%)
  local copies, waits for them, and re-layouts  22.6 us (6%)
    reduce_sum x8, other arithmetic, one_block(): jnp.sum(weigh_real * push_imag[None, :, :] + weigh_imag * push_real[None,...  76.7 us
    all_gather x1, waiting for transfers between devices, shards(): lax.all_gather(state_in_weight, SP, axis=0, tiled=True)  72.3 us
    all_gather x2, blocking collectives, gathered_once(): both, at, found = (lax.all_gather(jnp.concatenate(lines), axis), 0, {})  43.7 us
    all_to_all x1, blocking collectives, summed_on_arrival(): lax.all_to_all(cut_along(array, dim, devices), axis, 0, 0, tiled=True)  19.6 us
  transfers between devices with their start and end apart: 4, of which 2 were waited for; matrix products, arithmetic and copies ran while one was open for 39% of the time, Pallas kernels for 0%

commit v1 on v0

--- a/solution.py
+++ b/solution.py
@@ -228,7 +228,13 @@
         decay_rate, frequency, step_log, input_real, input_imag
     )
     doc_float = documents.astype(jnp.float32)
-    (driven_sum,) = add_rows((lax.all_gather(state_in_weight, SP, axis=0, tiled=True),))
+    (driven_sum,) = add_rows(
+        (
+            jnp.concatenate(
+                lax.all_to_all(jnp.stack([state_in_weight] * lax.axis_size(SP)), SP, 0, 0), axis=0
+            ),
+        )
+    )
     driven_wide = driven_sum.astype(jnp.bfloat16).astype(jnp.float32)
     split_rows = driven_wide.reshape(row_count, groups, group_size)
     backward = (row_count - 1 - jnp.arange(row_count)).astype(jnp.float32)[:, None]

time: 353 us -> 337 us (0.955)
  waiting for transfers between devices: 77.4 us -> 41.7 us
  starting transfers between devices: 2.03 us -> 20.2 us
    all_gather x1 -> x0, waiting for transfers between devices: 72.3 us -> none  [shards(): lax.all_gather(state_in_weight, SP, axis=0, tiled=True)]
    all_to_all x0 -> x1, waiting for transfers between devices: none -> 39.8 us  [shards(): lax.all_to_all(jnp.stack([state_in_weight] * lax.axis_size(SP)), SP, 0, 0)]
    all_to_all x0 -> x1, starting transfers between devices: none -> 15.6 us  [shards(): lax.all_to_all(jnp.stack([state_in_weight] * lax.axis_size(SP)), SP, 0, 0)]
    all_gather x2, blocking collectives: 43.7 us -> 40 us  [gathered_once(): both, at, found = (lax.all_gather(jnp.concatenate(lines), axis), 0, {})]
  transfers between devices with their start and end apart: 4 -> 4, of which waited for: 2 -> 2; matrix products, arithmetic and copies ran while one was open for 39% -> 41% of each run, Pallas kernels for 0% -> 0%
where the time goes in v1:
time: 337 us; the launch traced here: 336 us
  other arithmetic  95.4 us (28%)
  blocking collectives  64.5 us (19%)
  between operations  61.3 us (18%)
  waiting for transfers between devices  41.7 us (12%)
  matrix products  26.5 us (8%)
  local copies, waits for them, and re-layouts  25.1 us (7%)
  starting transfers between devices  20.2 us (6%)
    reduce_sum x8, other arithmetic, one_block(): jnp.sum(weigh_real * push_imag[None, :, :] + weigh_imag * push_real[None,...  76.7 us
    all_gather x2, blocking collectives, gathered_once(): both, at, found = (lax.all_gather(jnp.concatenate(lines), axis), 0, {})  40 us
    all_to_all x1, waiting for transfers between devices, shards(): lax.all_to_all(jnp.stack([state_in_weight] * lax.axis_size(SP)), SP, 0, 0)  39.8 us
    all_to_all x1, blocking collectives, summed_on_arrival(): lax.all_to_all(cut_along(array, dim, devices), axis, 0, 0, tiled=True)  21.4 us
    all_to_all x1, starting transfers between devices, shards(): lax.all_to_all(jnp.stack([state_in_weight] * lax.axis_size(SP)), SP, 0, 0)  15.6 us
    add x16, other arithmetic, one_block(): jnp.sum(weigh_real * push_imag[None, :, :] + weigh_imag * push_real[None,...  6.99 us
  transfers between devices with their start and end apart: 4, of which 2 were waited for; matrix products, arithmetic and copies ran while one was open for 41% of the time, Pallas kernels for 0%

profile of v1, /device:TPU:67, one launch (start us, length us, event | category | flops | bytes accessed | tf_op | source)
XLA Modules:
  0.0 335.7 jit_solution(5770984685856397555)
XLA Ops:
  6.5 1.4 pad_maximum_fusion.3
  8.0 2.3 stack.2
  10.4 15.6 %all-to-all-start = ((bf16[64,32,512]{2,1,0:T(8,128)(2,1)}), bf16[64,32,512]{2,1,0:T(8,128)(2,1)}, u32[]{:S(2)}, u32[]{:S(2)}) async-start(bf16[64,32,512]{2,1,0:T(8,128)(2,1)} %stack.2), calls=%async_computation | async-start | bytes 4194304 | tf_op jit(solution)/shard_map/all_to_all | solution.py:234
  26.1 0.6 pad_maximum_fusion.4
  26.8 0.6 fusion.204
  28.9 0.3 fusion.120
  29.4 0.6 fusion.203
  30.0 0.7 pad.14
  30.7 0.6 pad.15
  31.6 3.1 all_gather.21
  35.0 0.7 slice_compare_fusion.1
  35.7 0.6 compare_convert_fusion.3
  36.5 39.8 %all-to-all-done = bf16[64,32,512]{2,1,0:T(8,128)(2,1)} async-done(((bf16[64,32,512]{2,1,0:T(8,128)(2,1)}), bf16[64,32,512]{2,1,0:T(8,128)(2,1)}, u32[]{:S(2)}, u32[]{:S(2)}) %all-to-all-start) | async-done | bytes 2097184 | tf_op jit(solution)/shard_map/all_to_all | solution.py:234
  76.3 2.1 convolution_convert_fusion
  78.6 3.8 %fusion.79 = f32[32,64,16]{1,2,0:T(8,128)S(1)} fusion(bf16[128,32,16]{0,2,1:T(8,128)(2,1)S(1)} %bitcast.597, f32[32,64]{1,0:T(8,128)S(1)} %get-tuple-element.406, f32[128]{0:T(128)S(1)} %subtract_convert_fusion, f32[128]{0:T(128)S(1)} %get-tuple-element.414, f32[32,64]{1,0:T(8,128)S(1)} %get-tuple-element.405, f32[128]{0:T(128)S(1)} %fusion.178), kind=kOutput, calls=%fused_computation.77 | convolution fusion | flops 9437184 | bytes 280064 | tf_op jit(solution)/shard_map/tgp,tgh->gph/dot_general | solution.py:250
  82.4 4.4 %add_reduce_fusion = (f32[32,64]{1,0:T(8,128)S(1)}, f32[32,64]{1,0:T(8,128)S(1)}) fusion(f32[32,64,16]{1,2,0:T(8,128)S(1)} %get-tuple-element.304, f32[32,64,16]{1,2,0:T(8,128)S(1)} %get-tuple-element.253, f32[32,64,16]{1,2,0:T(8,128)S(1)} %fusion.79, bf16[128,32,16]{0,2,1:T(8,128)(2,1)S(1)} %bitcast.598, f32[32,64]{1,0:T(8,128)S(1)} %get-tuple-element.406, ...), kind=kOutput, calls=%fused_computation.109 | convolution fusion | flops 9695232 | bytes 558592 | tf_op jit(solution)/shard_map/tgp,tgh->gph/dot_general | solution.py:249
  87.0 22.1 %all-gather.2 = f32[8,6,2048]{2,1,0:T(8,128)S(1)} all-gather(f32[1,6,2048]{2,1,0:T(8,128)S(1)} %bitcast.594), channel_id=2, replica_groups=mesh['sp_0'=8,'sp_1'=8,'fs'=4,'tp'=2] {'sp_1'}, dimensions={0}, use_global_device_ids=true | all-gather | bytes 442368 | tf_op jit(solution)/shard_map/all_gather | solution.py:43
  109.3 0.6 fusion.201
  109.9 0.6 fusion.202
  136.5 17.8 %all-gather.3 = f32[8,6,2048]{2,1,0:T(8,128)S(1)} all-gather(f32[1,6,2048]{2,1,0:T(8,128)S(1)} %bitcast.595), channel_id=3, replica_groups=mesh['sp_0'=8,'sp_1'=8,'fs'=4,'tp'=2] {'sp_0'}, dimensions={0}, use_global_device_ids=true | all-gather | bytes 442368 | tf_op jit(solution)/shard_map/all_gather | solution.py:43
  154.5 0.6 fusion.200
  160.4 0.6 fusion.199
  177.4 112.4 %while.16 = (s32[]{:T(128)}, f32[2048]{0:T(1024)S(1)}, f32[2048]{0:T(1024)S(1)}, f32[8,16,512]{2,1,0:T(8,128)S(1)}, f32[8,16]{1,0:T(8,128)S(1)}, /*index=5*/bf16...) while((s32[]{:T(128)}, f32[2048]{0:T(1024)S(1)}, ...), condition=%wide.region_6.7_spmd.clone.clone, body=%wide.region_3.6_spmd.clone.clone.sunk | while | flops 12023074 | bytes 4772677 | solution.py:182
  177.6 0.2 convolution_bitcast_fusion.4
  178.5 9.6 %fusion.233 = (f32[16,2048]{1,0:T(8,128)S(1)}, f32[16,2048]{1,0:T(8,128)S(1)}) fusion(f32[2048]{0:T(1024)S(1)} %get-tuple-element.596, f32[16,16]{1,0:T(8,128)S(1)} %get-tuple-element.597, f32[2048]{0:T(1024)S(1)} %get-tuple-element.594, f32[16,16]{1,0:T(8,128)S(1)} %get-tuple-element.595, f32[16,2048]{1,0:T(8,128)S(1)} %mul.4733, ...), kind=kLoop, calls=%fused_computation.19.clone.1 | loop fusion | flops 7274496 | bytes 543744 | tf_op jit(solution)/shard_map/while/body/eval_jaxpr/reduce_sum | solution.py:171
  188.3 0.6 fusion.234
  190.1 0.6 slice.1072
  190.7 0.7 slice_add_fusion.18
  192.5 9.6 %fusion.233 = (f32[16,2048]{1,0:T(8,128)S(1)}, f32[16,2048]{1,0:T(8,128)S(1)}) fusion(f32[2048]{0:T(1024)S(1)} %get-tuple-element.596, f32[16,16]{1,0:T(8,128)S(1)} %get-tuple-element.597, f32[2048]{0:T(1024)S(1)} %get-tuple-element.594, f32[16,16]{1,0:T(8,128)S(1)} %get-tuple-element.595, f32[16,2048]{1,0:T(8,128)S(1)} %mul.4733, ...), kind=kLoop, calls=%fused_computation.19.clone.1 | loop fusion | flops 7274496 | bytes 543744 | tf_op jit(solution)/shard_map/while/body/eval_jaxpr/reduce_sum | solution.py:171
  202.4 0.6 fusion.234
  204.1 0.6 slice.1072
  204.8 0.7 slice_add_fusion.18
  206.6 9.6 %fusion.233 = (f32[16,2048]{1,0:T(8,128)S(1)}, f32[16,2048]{1,0:T(8,128)S(1)}) fusion(f32[2048]{0:T(1024)S(1)} %get-tuple-element.596, f32[16,16]{1,0:T(8,128)S(1)} %get-tuple-element.597, f32[2048]{0:T(1024)S(1)} %get-tuple-element.594, f32[16,16]{1,0:T(8,128)S(1)} %get-tuple-element.595, f32[16,2048]{1,0:T(8,128)S(1)} %mul.4733, ...), kind=kLoop, calls=%fused_computation.19.clone.1 | loop fusion | flops 7274496 | bytes 543744 | tf_op jit(solution)/shard_map/while/body/eval_jaxpr/reduce_sum | solution.py:171
  216.4 0.6 fusion.234
  218.2 0.6 slice.1072
  218.8 0.7 slice_add_fusion.18
  220.7 9.6 %fusion.233 = (f32[16,2048]{1,0:T(8,128)S(1)}, f32[16,2048]{1,0:T(8,128)S(1)}) fusion(f32[2048]{0:T(1024)S(1)} %get-tuple-element.596, f32[16,16]{1,0:T(8,128)S(1)} %get-tuple-element.597, f32[2048]{0:T(1024)S(1)} %get-tuple-element.594, f32[16,16]{1,0:T(8,128)S(1)} %get-tuple-element.595, f32[16,2048]{1,0:T(8,128)S(1)} %mul.4733, ...), kind=kLoop, calls=%fused_computation.19.clone.1 | loop fusion | flops 7274496 | bytes 543744 | tf_op jit(solution)/shard_map/while/body/eval_jaxpr/reduce_sum | solution.py:171
  230.5 0.6 fusion.234
  232.2 0.6 slice.1072
  232.9 0.7 slice_add_fusion.18
  234.7 9.6 %fusion.233 = (f32[16,2048]{1,0:T(8,128)S(1)}, f32[16,2048]{1,0:T(8,128)S(1)}) fusion(f32[2048]{0:T(1024)S(1)} %get-tuple-element.596, f32[16,16]{1,0:T(8,128)S(1)} %get-tuple-element.597, f32[2048]{0:T(1024)S(1)} %get-tuple-element.594, f32[16,16]{1,0:T(8,128)S(1)} %get-tuple-element.595, f32[16,2048]{1,0:T(8,128)S(1)} %mul.4733, ...), kind=kLoop, calls=%fused_computation.19.clone.1 | loop fusion | flops 7274496 | bytes 543744 | tf_op jit(solution)/shard_map/while/body/eval_jaxpr/reduce_sum | solution.py:171
  244.6 0.6 fusion.234
  246.3 0.6 slice.1072
  246.9 0.7 slice_add_fusion.18
  248.8 9.6 %fusion.233 = (f32[16,2048]{1,0:T(8,128)S(1)}, f32[16,2048]{1,0:T(8,128)S(1)}) fusion(f32[2048]{0:T(1024)S(1)} %get-tuple-element.596, f32[16,16]{1,0:T(8,128)S(1)} %get-tuple-element.597, f32[2048]{0:T(1024)S(1)} %get-tuple-element.594, f32[16,16]{1,0:T(8,128)S(1)} %get-tuple-element.595, f32[16,2048]{1,0:T(8,128)S(1)} %mul.4733, ...), kind=kLoop, calls=%fused_computation.19.clone.1 | loop fusion | flops 7274496 | bytes 543744 | tf_op jit(solution)/shard_map/while/body/eval_jaxpr/reduce_sum | solution.py:171
  258.6 0.6 fusion.234
  260.3 0.6 slice.1072
  261.0 0.7 slice_add_fusion.18
  262.8 9.6 %fusion.233 = (f32[16,2048]{1,0:T(8,128)S(1)}, f32[16,2048]{1,0:T(8,128)S(1)}) fusion(f32[2048]{0:T(1024)S(1)} %get-tuple-element.596, f32[16,16]{1,0:T(8,128)S(1)} %get-tuple-element.597, f32[2048]{0:T(1024)S(1)} %get-tuple-element.594, f32[16,16]{1,0:T(8,128)S(1)} %get-tuple-element.595, f32[16,2048]{1,0:T(8,128)S(1)} %mul.4733, ...), kind=kLoop, calls=%fused_computation.19.clone.1 | loop fusion | flops 7274496 | bytes 543744 | tf_op jit(solution)/shard_map/while/body/eval_jaxpr/reduce_sum | solution.py:171
  272.7 0.6 fusion.234
  274.4 0.6 slice.1072
  275.0 0.7 slice_add_fusion.18
  276.9 9.6 %fusion.233 = (f32[16,2048]{1,0:T(8,128)S(1)}, f32[16,2048]{1,0:T(8,128)S(1)}) fusion(f32[2048]{0:T(1024)S(1)} %get-tuple-element.596, f32[16,16]{1,0:T(8,128)S(1)} %get-tuple-element.597, f32[2048]{0:T(1024)S(1)} %get-tuple-element.594, f32[16,16]{1,0:T(8,128)S(1)} %get-tuple-element.595, f32[16,2048]{1,0:T(8,128)S(1)} %mul.4733, ...), kind=kLoop, calls=%fused_computation.19.clone.1 | loop fusion | flops 7274496 | bytes 543744 | tf_op jit(solution)/shard_map/while/body/eval_jaxpr/reduce_sum | solution.py:171
  286.7 0.6 fusion.234
  288.4 0.6 slice.1072
  289.1 0.7 slice_add_fusion.18
  290.0 2.1 fusion.67
  292.1 2.1 fusion.61
  294.3 4.6 %collective-permute-start = (bf16[2,512]{1,0:T(2,128)(2,1)S(1)}, bf16[2,512]{1,0:T(2,128)(2,1)S(1)}, u32[]{:S(2)}, u32[]{:S(2)}) collective-permute-start(bf16[2,512]{1,0:T(2,128)(2,1)S(1)} %broadcast_select_fusion.8), channel_id=1, source_target_pairs={{0,8},{8,16},{16,24},{24,32},{32,40},{40,48},{48,56},{56,64},{64,7... | collective-permute-start | bytes 6152 | tf_op jit(solution)/shard_map/ppermute | solution.py:77
  299.0 1.8 collective-permute-done
  300.7 3.5 %fusion.32 = f32[128,2048]{1,0:T(8,128)S(1)} fusion(bf16[2048,1024]{1,0:T(8,128)(2,1)} %all-gather.9.cloned.1.call-done, bf16[2048,1536]{1,0:T(8,128)(2,1)} %all-gather.7.cloned.1.call-done, bf16[128,512]{1,0:T(8,128)(2,1)S(1)} %fusion.61, bf16[2,512]{1,0:T(2,128)(2,1)S(1)} %collective-permute-done, f32[128]{0:T(128)S(1)} %get-tuple-element.415, ...), kind=kOutput, calls=%fused_computation.48 | convolution fusion | flops 539295744 | bytes 5916672 | tf_op jit(solution)/shard_map/dot_general | solution.py:322
  304.2 2.4 fusion.30
  306.6 21.4 %all_to_all.10 = bf16[2,64,2048]{2,1,0:T(8,128)(2,1)S(1)} all-to-all(bf16[2,64,2048]{2,1,0:T(8,128)(2,1)S(1)} %bitcast.587), channel_id=1, replica_groups=mesh['sp_0'=8,'sp_1'=8,'fs'=4,'tp'=2] {'tp'}, dimensions={0} | all-to-all | bytes 1048576 | tf_op jit(solution)/shard_map/all_to_all | solution.py:88
  328.0 0.8 reduce_sum.64
  (292 shorter events, 22.6 us)
Async XLA Ops:
  6.5 283.5 %all-gather.7.cloned.1.call-start = ((), (), s32[]{:S(2)}) async-start(), calls=%async_computation.2 | async-start | bytes 6389760 | tf_op jit(solution)/shard_map/all_gather | solution.py:70
  10.3 15.7 %copy-start.5 = (bf16[512,32]{0,1:T(8,128)(2,1)S(1)}, bf16[512,32]{0,1:T(8,128)(2,1)}, u32[]{:S(2)}) copy-start(bf16[512,32]{0,1:T(8,128)(2,1)} %param.37) | copy-start | bytes 98308
  10.3 15.7 %copy-start.6 = (bf16[512,32]{0,1:T(8,128)(2,1)S(1)}, bf16[512,32]{0,1:T(8,128)(2,1)}, u32[]{:S(2)}) copy-start(bf16[512,32]{0,1:T(8,128)(2,1)} %param.36) | copy-start | bytes 98308
  10.3 16.5 %copy-start.12 = (bf16[1024]{0:T(1024)(128)(2,1)S(1)}, bf16[1024]{0:T(1024)(128)(2,1)}, u32[]{:S(2)}) copy-start(bf16[1024]{0:T(1024)(128)(2,1)} %param.22) | copy-start | bytes 6148
  10.3 16.5 %copy-start.10 = (s32[128]{0:T(128)S(1)}, s32[128]{0:T(128)}, u32[]{:S(2)}) copy-start(s32[128]{0:T(128)} %param.21) | copy-start | bytes 1540
  10.3 18.5 %copy-start.13 = (f32[32]{0:T(128)S(1)}, f32[32]{0:T(128)}, u32[]{:S(2)}) copy-start(f32[32]{0:T(128)} %param.30) | copy-start | bytes 388
  10.3 18.5 %copy-start.7 = (f32[32,64]{1,0:T(8,128)S(1)}, f32[32,64]{1,0:T(8,128)}, u32[]{:S(2)}) copy-start(f32[32,64]{1,0:T(8,128)} %param.29) | copy-start | bytes 24580
  10.3 18.5 %copy-start.8 = (f32[32,64]{1,0:T(8,128)S(1)}, f32[32,64]{1,0:T(8,128)}, u32[]{:S(2)}) copy-start(f32[32,64]{1,0:T(8,128)} %param.28) | copy-start | bytes 24580
  10.3 21.1 %copy-start = (f32[32,16,64]{2,1,0:T(8,128)S(1)}, f32[32,16,64]{2,1,0:T(8,128)}, u32[]{:S(2)}) copy-start(f32[32,16,64]{2,1,0:T(8,128)} %param.33) | copy-start | bytes 393220
  10.4 21.2 %copy-start.1 = (f32[32,16,64]{2,1,0:T(8,128)S(1)}, f32[32,16,64]{2,1,0:T(8,128)}, u32[]{:S(2)}) copy-start(f32[32,16,64]{2,1,0:T(8,128)} %param.34) | copy-start | bytes 393220
  10.4 21.2 %copy-start.2 = (bf16[128,1024]{1,0:T(8,128)(2,1)S(1)}, bf16[128,1024]{1,0:T(8,128)(2,1)}, u32[]{:S(2)}) copy-start(bf16[128,1024]{1,0:T(8,128)(2,1)} %param.20) | copy-start | bytes 786436
  10.4 66.0 %all-to-all-start = ((bf16[64,32,512]{2,1,0:T(8,128)(2,1)}), bf16[64,32,512]{2,1,0:T(8,128)(2,1)}, u32[]{:S(2)}, u32[]{:S(2)}) async-start(bf16[64,32,512]{2,1,0:T(8,128)(2,1)} %stack.2), calls=%async_computation | async-start | bytes 4194304 | tf_op jit(solution)/shard_map/all_to_all | solution.py:234
  26.0 10.4 %copy-start.9 = (bf16[3,512]{1,0:T(4,128)(2,1)S(1)}, bf16[3,512]{1,0:T(4,128)(2,1)}, u32[]{:S(2)}) copy-start(bf16[3,512]{1,0:T(4,128)(2,1)} %param.26) | copy-start | bytes 9220
  26.0 10.4 %copy-start.3 = (f32[32,64,16]{1,2,0:T(8,128)S(1)}, f32[32,64,16]{1,2,0:T(8,128)}, u32[]{:S(2)}) copy-start(f32[32,64,16]{1,2,0:T(8,128)} %param.32) | copy-start | bytes 393220
  26.0 10.4 %copy-start.4 = (f32[32,64,16]{1,2,0:T(8,128)S(1)}, f32[32,64,16]{1,2,0:T(8,128)}, u32[]{:S(2)}) copy-start(f32[32,64,16]{1,2,0:T(8,128)} %param.31) | copy-start | bytes 393220
  26.0 273.0 %all-gather.9.cloned.1.call-start = ((), (), s32[]{:S(2)}) async-start(), calls=%async_computation.3 | async-start | bytes 4259840 | tf_op jit(solution)/shard_map/all_gather | solution.py:19
  177.4 112.5 %copy-start.11 = (f32[512]{0:T(512)S(1)}, f32[512]{0:T(512)}, u32[]{:S(2)}) copy-start(f32[512]{0:T(512)} %param.35) | copy-start | bytes 6148
  294.3 6.4 %collective-permute-start = (bf16[2,512]{1,0:T(2,128)(2,1)S(1)}, bf16[2,512]{1,0:T(2,128)(2,1)S(1)}, u32[]{:S(2)}, u32[]{:S(2)}) collective-permute-start(bf16[2,512]{1,0:T(2,128)(2,1)S(1)} %broadcast_select_fusion.8), channel_id=1, source_target_pairs={{0,8},{8,16},{16,24},{24,32},{32,40},{40,48},{48,56},{56,64},{64,7... | collective-permute-start | bytes 6152 | tf_op jit(solution)/shard_map/ppermute | solution.py:77
Sparse Core Ops, SparseCore 0:
  10.3 128.1 all-gather.6
  141.6 81.2 all-gather.8
